TPU v7x, 32 devices: a whole 2x2x4 slice. The times are simulated.
32 devices in a mesh: gr: 2 (over x), fs: 8 (over z, y), tp: 2 (over core).
Axes of the slice: x: 2, y: 2, z: 4, core: 2. Of those that a mesh axis runs over, the one named last changes fastest.
Arguments:
- tokens: bfloat16 [2816, 2048], P(('gr', 'fs')), may hold values from -6 to 6
- expert_ids: int32 [2816, 8], P(('gr', 'fs')), may hold values from 0 to 15, all different within a row; in each aligned block of 176 rows (0 to 175, 176 to 351, ...) at most 110 rows name the same one
- route_weight: float32 [2816, 8], P(('gr', 'fs')), may hold values from 0.05 to 1
- norm_gain: float32 [2048], P('tp'), may hold values from 0.1 to 1.9
- expert_gate: float32 [16, 512, 2048], P('gr', 'fs', 'tp'), may hold values from -0.125 to 0.125
- expert_up: float32 [16, 512, 2048], P('gr', 'fs', 'tp'), may hold values from -0.125 to 0.125
- expert_down: float32 [16, 512, 2048], P('gr', 'fs', 'tp'), may hold values from -0.25 to 0.25
- shared_gate: float32 [512, 2048], P('fs', 'tp'), may hold values from -0.125 to 0.125
- shared_up: float32 [512, 2048], P('fs', 'tp'), may hold values from -0.125 to 0.125
- shared_down: float32 [512, 2048], P('fs', 'tp'), may hold values from -0.25 to 0.25
Outputs:
- mixed: bfloat16 [2816, 2048], P(('gr', 'fs'), 'tp')
- new_gate: bfloat16 [2, 8, 512, 2048], P(None, 'fs', None, 'tp')
- new_up: bfloat16 [2, 8, 512, 2048], P(None, 'fs', None, 'tp')
- new_down: bfloat16 [2, 8, 512, 2048], P(None, 'fs', None, 'tp')
- new_shared_gate: bfloat16 [512, 2048], P(None, 'tp')
- new_shared_up: bfloat16 [512, 2048], P(None, 'tp')
- new_shared_down: bfloat16 [512, 2048], P(None, 'tp')
Inputs may be any that keep to these rules, and one draw needn't show every extreme that they name: `expert_ids`: each row names 8 different experts; within each aligned block of 176 rows no expert is named by more than 110 rows, a bound that some block reaches.
All inputs are finite; a program needn't handle non-finite values.
Results may differ from a plain program's by a relative error of at most 0.022.
Values may be sent and summed in bfloat16 or wider, within the bound.
A program may use at most 128 MiB of HBM per device.

v0:
```python
import jax
import jax.numpy as jnp
from jax import lax
from jax.sharding import PartitionSpec as P

route_scale = 2.5
norm_eps = 1e-06


def fold_gain(weight, gain):
    return (weight * gain).astype(jnp.bfloat16)


def body(
    tokens,
    expert_ids,
    route_weight,
    norm_gain,
    expert_gate,
    expert_up,
    expert_down,
    shared_gate,
    shared_up,
    shared_down,
):
    group_count = lax.axis_size("gr")
    shard_count = lax.axis_size("fs")
    column_count = lax.axis_size("tp")
    tok_rows = tokens.shape[0]
    col_width = expert_gate.shape[2]
    top_count = expert_ids.shape[1]
    hidden = expert_gate.shape[1] * shard_count
    shared_hidden = shared_gate.shape[0] * shard_count
    experts = group_count * shard_count
    capacity = tok_rows * top_count * 5 // (4 * experts)
    gate_round = fold_gain(expert_gate, norm_gain)
    up_round = fold_gain(expert_up, norm_gain)
    down_round = expert_down.astype(jnp.bfloat16)
    moved = (
        lax.all_to_all(gate_round, "fs", split_axis=0, concat_axis=1, tiled=True),
        lax.all_to_all(up_round, "fs", split_axis=0, concat_axis=1, tiled=True),
        lax.all_to_all(down_round, "fs", split_axis=0, concat_axis=1, tiled=True),
    )
    whole = (
        lax.all_gather(moved[0], "gr", axis=0, tiled=True),
        lax.all_gather(moved[1], "gr", axis=0, tiled=True),
        lax.all_gather(moved[2], "gr", axis=0, tiled=True),
    )
    new_gate, new_up, new_down = tuple(
        (matrix.reshape(group_count, 1, hidden, col_width) for matrix in whole)
    )
    new_shared_gate, new_shared_up, new_shared_down = (
        lax.all_gather(fold_gain(shared_gate, norm_gain), "fs", axis=0, tiled=True),
        lax.all_gather(fold_gain(shared_up, norm_gain), "fs", axis=0, tiled=True),
        lax.all_gather(shared_down.astype(jnp.bfloat16), "fs", axis=0, tiled=True),
    )
    tok_float = tokens.astype(jnp.float32)
    normed = (
        tok_float * lax.rsqrt(jnp.mean(tok_float * tok_float, axis=1, keepdims=True) + norm_eps)
    ).astype(jnp.bfloat16)
    normed_cols = lax.dynamic_slice_in_dim(normed, lax.axis_index("tp") * col_width, col_width, 1)
    flat_expert = expert_ids.reshape(-1)
    one_hot = (flat_expert[:, None] == jnp.arange(experts, dtype=jnp.int32)[None, :]).astype(
        jnp.int32
    )
    running = jnp.cumsum(one_hot, axis=0)
    rank = jnp.sum((running - one_hot) * one_hot, axis=1)
    dest = flat_expert * capacity + rank
    token_of = jnp.arange(tok_rows * top_count, dtype=jnp.int32) // top_count
    slot_token = jnp.full((experts * capacity,), tok_rows, jnp.int32).at[dest].set(token_of)
    padded = jnp.concatenate([normed_cols, jnp.zeros((1, col_width), jnp.bfloat16)], axis=0)
    outgoing = padded[slot_token].reshape(group_count, shard_count, capacity, col_width)
    arrived = lax.all_to_all(outgoing, "fs", split_axis=1, concat_axis=1, tiled=True)
    slot_rows = arrived.reshape(group_count, shard_count * capacity, col_width)
    pair_weight = jnp.stack([new_gate[:, 0], new_up[:, 0]], axis=2).reshape(
        group_count, 2 * hidden, col_width
    )
    rows_weight = pair_weight
    term = jnp.einsum("ihd,ird->hir", rows_weight, slot_rows, preferred_element_type=jnp.float32)
    pair_sum = lax.psum_scatter(
        term.reshape(
            2 * hidden // column_count * lax.axis_size("tp"), group_count * shard_count * capacity
        ).astype(jnp.bfloat16),
        "tp",
        scatter_dimension=0,
        tiled=True,
    ).astype(jnp.float32)
    pair_sum = pair_sum.reshape(hidden // column_count, 2, group_count, shard_count * capacity)
    activation = (jax.nn.silu(pair_sum[:, 0]) * pair_sum[:, 1]).astype(jnp.bfloat16)
    down_local = new_down[:, 0]
    rows_down = down_local
    slot_out = jnp.einsum(
        "hir,ihd->ird",
        lax.all_gather(activation, "tp", axis=0, tiled=True),
        rows_down,
        preferred_element_type=jnp.float32,
    )
    returning = slot_out.astype(jnp.bfloat16).reshape(group_count, shard_count, capacity, col_width)
    returned = lax.all_to_all(returning, "fs", split_axis=1, concat_axis=1, tiled=True)
    result_rows = returned.reshape(experts * capacity, col_width)
    picked = result_rows[dest].reshape(tok_rows, top_count, col_width).astype(jnp.float32)
    share = route_weight / jnp.sum(route_weight, axis=1, keepdims=True) * route_scale
    routed = jnp.sum(share[:, :, None] * picked, axis=1)
    shared_pair = jnp.stack([new_shared_gate, new_shared_up], axis=1).reshape(
        2 * shared_hidden, col_width
    )
    rows_weight = shared_pair
    shared_sum = lax.psum_scatter(
        lax.dot_general(
            rows_weight, normed_cols, (((1,), (1,)), ((), ())), preferred_element_type=jnp.float32
        ).astype(jnp.bfloat16),
        "tp",
        scatter_dimension=0,
        tiled=True,
    ).astype(jnp.float32)
    shared_sum = shared_sum.reshape(shared_hidden // column_count, 2, tok_rows)
    shared_act = (jax.nn.silu(shared_sum[:, 0]) * shared_sum[:, 1]).astype(jnp.bfloat16)
    rows_down = new_shared_down
    shared_out = lax.dot_general(
        lax.all_gather(shared_act, "tp", axis=0, tiled=True),
        rows_down,
        (((0,), (0,)), ((), ())),
        preferred_element_type=jnp.float32,
    )
    mixed = (shared_out + routed).astype(jnp.bfloat16)
    return (mixed, new_gate, new_up, new_down, new_shared_gate, new_shared_up, new_shared_down)


def solution(mesh):
    placed = (
        P(("gr", "fs"), None),
        P(("gr", "fs"), None),
        P(("gr", "fs"), None),
        P("tp"),
        P("gr", "fs", "tp"),
        P("gr", "fs", "tp"),
        P("gr", "fs", "tp"),
        P("fs", "tp"),
        P("fs", "tp"),
        P("fs", "tp"),
    )
    return jax.shard_map(
        body,
        mesh=mesh,
        in_specs=placed,
        out_specs=(
            P(("gr", "fs"), "tp"),
            P(None, "fs", None, "tp"),
            P(None, "fs", None, "tp"),
            P(None, "fs", None, "tp"),
            P(None, "tp"),
            P(None, "tp"),
            P(None, "tp"),
        ),
        check_vma=False,
    )
```

profile of v0, /device:TPU:0, one launch (start us, length us, event | category | flops | bytes accessed | tf_op | source)
XLA Modules:
  0.0 498.2 jit_solution(3929009726196123222)
XLA Ops:
  7.2 4.0 multiply_convert_fusion.1
  11.2 7.4 %all-to-all-start.2 = ((bf16[8,64,1024]{2,1,0:T(8,128)(2,1)}), bf16[8,64,1024]{2,1,0:T(8,128)(2,1)S(1)}, u32[]{:S(2)}, u32[]{:S(2)}) async-start(bf16[8,64,1024]{2,1,0:T(8,128)(2,1)} %get-tuple-element.42), calls=%async_computation.3 | async-start | bytes 2097152 | tf_op jit(solution)/shard_map/all_to_all | solution.py:41
  19.0 1.3 convert_element_type.65
  20.5 23.9 %all-to-all-done.2 = bf16[8,64,1024]{2,1,0:T(8,128)(2,1)S(1)} async-done(((bf16[8,64,1024]{2,1,0:T(8,128)(2,1)}), bf16[8,64,1024]{2,1,0:T(8,128)(2,1)S(1)}, u32[]{:S(2)}, u32[]{:S(2)}) %all-to-all-start.2) | async-done | bytes 1048608 | tf_op jit(solution)/shard_map/all_to_all | solution.py:41
  44.4 3.6 all-to-all-start.1
  48.0 4.5 reduce-window.6
  53.4 1.2 fusion.11
  54.9 7.6 %scatter_custom_fusion = s32[1760]{0:T(1024)S(1)} fusion(s32[1408]{0:T(1024)S(1)} %fusion.23, s32[1408]{0:T(1024)S(1)} %add_select_fusion, s32[]{:T(128)} %constant.49.clone.1), kind=kCustom, calls=%fused_computation.58 | custom fusion | bytes 7044 | tf_op jit(solution)/shard_map/scatter | solution.py:70
  62.5 6.6 %gather_fusion = bf16[1760,1024]{1,0:T(8,128)(2,1)} fusion(bf16[177,1024]{1,0:T(8,128)(2,1)S(1)} %concatenate.3, s32[2048]{0:T(1024)S(1)} %pad_clamp_fusion.1), kind=kCustom, calls=%fused_computation | custom fusion | bytes 7216000 | tf_op jit(solution)/shard_map/gather | solution.py:72
  69.1 4.8 reshape.129
  73.8 7.6 %copy.55 = bf16[2,8,110,1024]{3,0,2,1:T(2,128)(2,1)} copy(bf16[2,8,110,1024]{3,2,1,0:T(8,128)(2,1)} %reshape.129) | data formatting | bytes 7208960 | tf_op jit(solution)/shard_map/reshape | solution.py:72
  82.4 6.0 %all-to-all-start = ((bf16[2,8,110,1024]{3,0,2,1:T(2,128)(2,1)}), bf16[2,8,110,1024]{3,0,2,1:T(2,128)(2,1)}, u32[]{:S(2)}, u32[]{:S(2)}) async-start(bf16[2,8,110,1024]{3,0,2,1:T(2,128)(2,1)} %copy.55), calls=%async_computation.1 | async-start | bytes 7208960 | tf_op jit(solution)/shard_map/all_to_all | solution.py:73
  90.1 35.7 %all-gather.16.cloned.1.call-done = bf16[2,512,1024]{2,1,0:T(8,128)(2,1)} async-done(((bf16[1,512,1024]{2,1,0:T(8,128)(2,1)}), bf16[2,512,1024]{2,1,0:T(8,128)(2,1)}) %all-gather.16.cloned.1.call-update) | async-done | bytes 2097168 | tf_op jit(solution)/shard_map/all_gather | solution.py:46
  125.8 35.2 %all-gather.14.cloned.1.call-done = bf16[2,512,1024]{2,1,0:T(8,128)(2,1)} async-done(((bf16[1,512,1024]{2,1,0:T(8,128)(2,1)}), bf16[2,512,1024]{2,1,0:T(8,128)(2,1)}) %all-gather.14.cloned.1.call-update) | async-done | bytes 2097168 | tf_op jit(solution)/shard_map/all_gather | solution.py:45
  161.1 2.6 pad_maximum_fusion
  163.7 6.3 %copy.57 = bf16[2,512,2,1024]{3,2,1,0:T(2,128)(2,1)} copy(bf16[2,512,2,1024]{3,1,0,2:T(8,128)(2,1)S(1)} %pad_maximum_fusion) | data formatting | bytes 8388608 | tf_op jit(solution)/shard_map/stack | solution.py:75
  170.0 7.2 %reshape.131 = bf16[2,1024,1024]{2,1,0:T(8,128)(2,1)} reshape(bf16[2,512,2,1024]{3,2,1,0:T(2,128)(2,1)} %copy.57) | data formatting | bytes 8388608 | tf_op jit(solution)/shard_map/reshape | solution.py:75
  177.2 9.0 %fusion.3 = bf16[2,880,1024]{2,1,0:T(8,128)(2,1)} fusion(bf16[2,1024,1024]{2,1,0:T(8,128)(2,1)} %reshape.131, bf16[2,880,1024]{2,0,1:T(2,128)(2,1)} %bitcast.5), kind=kOutput, calls=%fused_computation.8 | convolution fusion | flops 3692789760 | bytes 11403264 | tf_op jit(solution)/shard_map/ihd,ird->hir/dot_general | solution.py:79
  186.1 5.8 %copy.58 = bf16[1024,1760]{1,0:T(8,128)(2,1)} copy(bf16[1024,1760]{0,1:T(8,128)(2,1)} %bitcast.93) | data formatting | bytes 7208960 | tf_op jit(solution)/shard_map/convert_element_type | solution.py:83
  192.1 1.5 copy-done.8
  193.7 31.0 %all_to_all.46 = bf16[8,64,1024]{2,1,0:T(8,128)(2,1)} all-to-all(bf16[8,64,1024]{2,1,0:T(8,128)(2,1)S(1)} %convert_element_type.78), channel_id=1, replica_groups=mesh['gr'=2,'fs'=8,'tp'=2] {'fs'}, dimensions={0} | all-to-all | bytes 2097152 | tf_op jit(solution)/shard_map/all_to_all | solution.py:42
  225.1 5.6 %reshape.142 = f32[256,2,2,880]{3,2,1,0:T(2,128)} reshape(bf16[512,1760]{1,0:T(8,128)(2,1)} %reduce-scatter.5.cloned.1.call-done) | data formatting | bytes 5406720 | tf_op jit(solution)/shard_map/reshape | solution.py:88
  230.6 4.8 fusion.26
  235.4 3.9 copy.69
  239.4 2.5 copy.68
  241.9 3.5 fusion.6
  246.3 9.8 %all-gather.20.cloned.1.call-done = bf16[2,512,1024]{2,1,0:T(8,128)(2,1)} async-done(((bf16[1,512,1024]{2,1,0:T(8,128)(2,1)}), bf16[2,512,1024]{2,1,0:T(8,128)(2,1)}) %all-gather.20.cloned.1.call-update) | async-done | bytes 2097168 | tf_op jit(solution)/shard_map/all_gather | solution.py:47
  256.1 11.7 %all-gather.18.cloned.1.call-done = bf16[512,2,880]{0,2,1:T(8,128)(2,1)} async-done(((bf16[256,2,880]{0,2,1:T(8,128)(2,1)}), bf16[512,2,880]{0,2,1:T(8,128)(2,1)}) %all-gather.18.cloned.1.call-update) | async-done | bytes 1802256 | tf_op jit(solution)/shard_map/all_gather | solution.py:94
  267.8 4.2 convolution_convert_fusion
  272.0 5.5 %copy.67 = bf16[2,880,1024]{2,0,1:T(2,128)(2,1)} copy(bf16[2,880,1024]{2,1,0:T(8,128)(2,1)S(1)} %convolution_convert_fusion) | data formatting | bytes 7208960 | tf_op jit(solution)/shard_map/reshape | solution.py:98
  277.5 5.9 %all-to-all-start.4 = ((bf16[2,8,110,1024]{3,0,2,1:T(2,128)(2,1)}), bf16[2,8,110,1024]{3,0,2,1:T(2,128)(2,1)}, u32[]{:S(2)}, u32[]{:S(2)}) async-start(bf16[2,8,110,1024]{3,0,2,1:T(2,128)(2,1)} %bitcast.83), calls=%async_computation.6 | async-start | bytes 7208960 | tf_op jit(solution)/shard_map/all_to_all | solution.py:99
  285.2 75.8 %all-gather.10.cloned.1.call-done = bf16[512,1024]{1,0:T(8,128)(2,1)} async-done(((bf16[64,1024]{1,0:T(8,128)(2,1)}), bf16[512,1024]{1,0:T(8,128)(2,1)}) %all-gather.10.cloned.1.call-update) | async-done | bytes 1048592 | tf_op jit(solution)/shard_map/all_gather | solution.py:54
  361.0 42.5 %all-gather.8.cloned.1.call-done = bf16[512,1024]{1,0:T(8,128)(2,1)} async-done(((bf16[64,1024]{1,0:T(8,128)(2,1)}), bf16[512,1024]{1,0:T(8,128)(2,1)}) %all-gather.8.cloned.1.call-update) | async-done | bytes 1048592 | tf_op jit(solution)/shard_map/all_gather | solution.py:53
  403.5 1.7 pad_maximum_fusion.1
  405.3 2.2 copy.47
  407.4 2.2 reshape.125
  409.7 3.2 convolution_convert_fusion.1
  413.0 32.2 %all-gather.12.cloned.1.call-done = bf16[512,1024]{1,0:T(8,128)(2,1)} async-done(((bf16[64,1024]{1,0:T(8,128)(2,1)}), bf16[512,1024]{1,0:T(8,128)(2,1)}) %all-gather.12.cloned.1.call-update) | async-done | bytes 1048592 | tf_op jit(solution)/shard_map/all_gather | solution.py:55
  445.3 9.4 %reduce-scatter.3.cloned.1.call-done = bf16[512,176]{0,1:T(8,128)(2,1)} async-done(((bf16[1024,176]{0,1:T(8,128)(2,1)}), bf16[512,176]{0,1:T(8,128)(2,1)}) %reduce-scatter.3.cloned.1.call-update) | async-done | bytes 180240 | tf_op jit(solution)/shard_map/reduce_scatter | solution.py:108
  456.7 1.9 all_gather.26
  458.7 5.0 copy.62
  463.6 4.8 reshape.135
  468.4 9.7 %gather_fusion.1 = bf16[1408,1024]{1,0:T(8,128)(2,1)S(1)} fusion(bf16[1760,1024]{1,0:T(8,128)(2,1)} %reshape.135, s32[2048]{0:T(1024)S(1)} %pad_clamp_fusion), kind=kCustom, calls=%fused_computation.1 | custom fusion | bytes 5772800 | tf_op jit(solution)/shard_map/gather | solution.py:101
  478.2 1.7 fusion
  479.9 1.1 fusion.10
  481.0 1.3 copy.82
  483.4 1.3 copy.83
  485.7 1.3 copy.84
  (87 shorter events, 15.8 us)
Async XLA Ops:
  11.2 7.4 %copy-start.13 = (s32[176,8]{0,1:T(8,128)S(1)}, s32[176,8]{0,1:T(8,128)}, u32[]{:S(2)}) copy-start(s32[176,8]{0,1:T(8,128)} %param.11) | copy-start | bytes 16900
  11.2 7.8 %copy-start.7 = (bf16[176,2048]{1,0:T(8,128)(2,1)S(1)}, bf16[176,2048]{1,0:T(8,128)(2,1)}, u32[]{:S(2)}) copy-start(bf16[176,2048]{1,0:T(8,128)(2,1)} %param.10) | copy-start | bytes 2162692
  11.2 33.2 %all-to-all-start.2 = ((bf16[8,64,1024]{2,1,0:T(8,128)(2,1)}), bf16[8,64,1024]{2,1,0:T(8,128)(2,1)S(1)}, u32[]{:S(2)}, u32[]{:S(2)}) async-start(bf16[8,64,1024]{2,1,0:T(8,128)(2,1)} %get-tuple-element.42), calls=%async_computation.3 | async-start | bytes 2097152 | tf_op jit(solution)/shard_map/all_to_all | solution.py:41
  44.4 10.2 %copy-start.2 = (bf16[8,64,1024]{2,1,0:T(8,128)(2,1)}, bf16[8,64,1024]{2,1,0:T(8,128)(2,1)S(1)}, u32[]{:S(2)}) copy-start(bf16[8,64,1024]{2,1,0:T(8,128)(2,1)S(1)} %all-to-all-done.2) | copy-start | bytes 3145732
  44.4 37.0 %all-to-all-start.1 = ((bf16[8,64,1024]{2,1,0:T(8,128)(2,1)}), bf16[8,64,1024]{2,1,0:T(8,128)(2,1)S(1)}, u32[]{:S(2)}, u32[]{:S(2)}) async-start(bf16[8,64,1024]{2,1,0:T(8,128)(2,1)} %get-tuple-element.41), calls=%async_computation.2 | async-start | bytes 2097152 | tf_op jit(solution)/shard_map/all_to_all | solution.py:40
  81.4 1.0 copy-start.4
  82.4 94.8 %all-to-all-start = ((bf16[2,8,110,1024]{3,0,2,1:T(2,128)(2,1)}), bf16[2,8,110,1024]{3,0,2,1:T(2,128)(2,1)}, u32[]{:S(2)}, u32[]{:S(2)}) async-start(bf16[2,8,110,1024]{3,0,2,1:T(2,128)(2,1)} %copy.55), calls=%async_computation.1 | async-start | bytes 7208960 | tf_op jit(solution)/shard_map/all_to_all | solution.py:73
  88.4 37.4 %all-gather.16.cloned.1.call-start = ((), (), s32[]{:S(2)}) async-start(), calls=%async_computation.12 | async-start | bytes 3145728 | tf_op jit(solution)/shard_map/all_gather | solution.py:46
  89.1 72.0 %all-gather.14.cloned.1.call-start = ((), (), s32[]{:S(2)}) async-start(), calls=%async_computation.11 | async-start | bytes 3145728 | tf_op jit(solution)/shard_map/all_gather | solution.py:45
  89.8 135.2 %reduce-scatter.5.cloned.1.call-start = ((), (), s32[]{:S(2)}) async-start(), calls=%async_computation.13 | async-start | bytes 5505024 | tf_op jit(solution)/shard_map/reduce_scatter | solution.py:80
  192.0 1.6 copy-start.8
  192.0 64.1 %all-gather.20.cloned.1.call-start = ((), (), s32[]{:S(2)}) async-start(), calls=%async_computation.15 | async-start | bytes 3145728 | tf_op jit(solution)/shard_map/all_gather | solution.py:47
  224.8 43.0 %all-gather.18.cloned.1.call-start = ((), (), s32[]{:S(2)}) async-start(), calls=%async_computation.14 | async-start | bytes 2703360 | tf_op jit(solution)/shard_map/all_gather | solution.py:94
  241.9 3.6 copy-start.10
  241.9 3.6 copy-start.11
  241.9 3.6 copy-start.15
  245.4 115.6 %all-gather.10.cloned.1.call-start = ((), (), s32[]{:S(2)}) async-start(), calls=%async_computation.8 | async-start | bytes 1179648 | tf_op jit(solution)/shard_map/all_gather | solution.py:54
  277.5 6.7 %copy-start.12 = (f32[64,1024]{1,0:T(8,128)S(1)}, f32[64,1024]{1,0:T(8,128)}, u32[]{:S(2)}) copy-start(f32[64,1024]{1,0:T(8,128)} %param.19) | copy-start | bytes 786436
  277.5 181.2 %all-to-all-start.4 = ((bf16[2,8,110,1024]{3,0,2,1:T(2,128)(2,1)}), bf16[2,8,110,1024]{3,0,2,1:T(2,128)(2,1)}, u32[]{:S(2)}, u32[]{:S(2)}) async-start(bf16[2,8,110,1024]{3,0,2,1:T(2,128)(2,1)} %bitcast.83), calls=%async_computation.6 | async-start | bytes 7208960 | tf_op jit(solution)/shard_map/all_to_all | solution.py:99
  283.4 120.1 %all-gather.8.cloned.1.call-start = ((), (), s32[]{:S(2)}) async-start(), calls=%async_computation.7 | async-start | bytes 1179648 | tf_op jit(solution)/shard_map/all_gather | solution.py:53
  284.2 161.1 %all-gather.12.cloned.1.call-start = ((), (), s32[]{:S(2)}) async-start(), calls=%async_computation.10 | async-start | bytes 1179648 | tf_op jit(solution)/shard_map/all_gather | solution.py:55
  284.9 169.7 %reduce-scatter.3.cloned.1.call-start = ((), (), s32[]{:S(2)}) async-start(), calls=%async_computation.9 | async-start | bytes 540672 | tf_op jit(solution)/shard_map/reduce_scatter | solution.py:108
  409.6 3.2 copy-start.14
  478.1 1.8 copy-start.3
  478.1 2.9 copy-start.1
  481.0 2.3 copy-start
  483.4 2.3 copy-start.9
  485.7 2.0 copy-start.6
  487.7 1.6 copy-start.5
Sparse Core Ops, SparseCore 0:
  91.3 34.4 all-gather.15
  127.9 33.0 all-gather.13
  192.1 11.8 reduce-scatter.4
  224.9 31.1 all-gather.19
  258.1 9.7 all-gather.17
  270.4 90.5 all-gather.9
  363.7 39.7 all-gather.7
  406.2 38.9 all-gather.11
  448.1 6.5 reduce-scatter.2
where the time goes:
time: 506 us; the launch traced here: 498 us
  waiting for transfers between devices  279 us (55%)
  local copies, waits for them, and re-layouts  108 us (21%)
  blocking collectives  33 us (7%)
  starting transfers between devices  24 us (5%)
  other arithmetic  22.9 us (5%)
  matrix products  17.4 us (3%)
  between operations  14.6 us (3%)
    all_gather x1, waiting for transfers between devices, body(): lax.all_gather(fold_gain(shared_up, norm_gain), 'fs', axis=0, tiled=True)  75.8 us
    all_gather x1, waiting for transfers between devices, body(): lax.all_gather(fold_gain(shared_gate, norm_gain), 'fs', axis=0, tiled=True)  42.5 us
    all_gather x1, waiting for transfers between devices, body(): lax.all_gather(moved[1], 'gr', axis=0, tiled=True)  35.7 us
    all_gather x1, waiting for transfers between devices, body(): lax.all_gather(moved[0], 'gr', axis=0, tiled=True)  35.2 us
    all_gather x1, waiting for transfers between devices, body(): lax.all_gather(shared_down.astype(jnp.bfloat16), 'fs', axis=0, tiled=True)  32.2 us
    all_to_all x1, blocking collectives, body(): lax.all_to_all(down_round, 'fs', split_axis=0, concat_axis=1, tiled=True)  31 us
    all_to_all x1, waiting for transfers between devices, body(): lax.all_to_all(up_round, 'fs', split_axis=0, concat_axis=1, tiled=True)  23.9 us
    unnamed x41, local copies, waits for them, and re-layouts  19.3 us
  transfers between devices with their start and end apart: 13, of which 9 were waited for; matrix products, arithmetic and copies ran while one was open for 19% of the time, Pallas kernels for 0%

commit v1 on v0

v1 whole, which is shorter than its diff:
```python
import functools

import jax
import jax.numpy as jnp
from jax import lax
from jax.experimental import pallas as pl
from jax.experimental.pallas import tpu as pltpu
from jax.sharding import PartitionSpec as P

route_scale = 2.5
norm_eps = 1e-06
vmem_bytes = 67043328


def fold_gain(weight, gain):
    return (weight * gain).astype(jnp.bfloat16)


def silu(v):
    return v / (1.0 + jnp.exp(-v))


def handover(
    dims,
    tok,
    w0,
    w1,
    w2,
    s0,
    s1,
    s2,
    mixed,
    o0,
    o1,
    o2,
    q0,
    q1,
    q2,
    n0,
    n1,
    n2,
    h0,
    h1,
    h2,
    xs,
    pout,
    pin,
    act,
    oz,
    rety,
    ret,
    psh,
    pshin,
    local_sem,
    out_sem,
    tok_send,
    tok_recv,
    w_send,
    w_recv,
    x_send,
    x_recv,
    sh_send,
    sh_recv,
    shx_send,
    shx_recv,
    p_send,
    p_recv,
    a_send,
    a_recv,
    ry_send,
    ry_recv,
    r_send,
    r_recv,
    ps_send,
    ps_recv,
):
    G, S, TP, T, C, H, F, SF, slots, Y = dims
    Z = S // Y
    E = G * S
    SH = SF * S
    NB = S // TP
    NH = NB * T
    gi, si, ti = lax.axis_index("gr"), lax.axis_index("fs"), lax.axis_index("tp")
    zi, yi = si // Y, lax.rem(si, Y)
    w, new, sh, shn = (w0, w1, w2), (n0, n1, n2), (s0, s1, s2), (h0, h1, h2)
    outs, shouts = (o0, o1, o2), (q0, q1, q2)

    def rdma(src, dst, ssem, rsem, dev):
        return pltpu.make_async_remote_copy(
            src_ref=src,
            dst_ref=dst,
            send_sem=ssem,
            recv_sem=rsem,
            device_id=dev,
            device_id_type=pl.DeviceIdType.MESH,
        )

    def rows(start, step, size):
        return pl.ds(pl.multiple_of(start * step, step), size)

    def each(lo, hi, fn):
        def step(i, c):
            fn(i)
            return c

        lax.fori_loop(lo, hi, step, 0)

    def fs_peer(k):
        return lax.rem(si + k, S)

    def fs_from(k):
        return lax.rem(si + S - k, S)

    def gr_peer(k):
        return lax.rem(gi + k, G)

    def tp_peer(k):
        return lax.rem(ti + k, TP)

    barrier = pltpu.get_barrier_semaphore()

    def greet(axis, peer, n):
        each(
            1,
            n,
            lambda k: pl.semaphore_signal(
                barrier,
                inc=1,
                device_id={axis: peer(k)},
                device_id_type=pl.DeviceIdType.MESH,
            ),
        )

    greet("fs", fs_peer, S)
    greet("gr", gr_peer, G)
    greet("tp", tp_peer, TP)
    pl.semaphore_wait(barrier, S + G + TP - 3)

    def w_copy(m, d, s):
        return rdma(
            w[m].at[d], new[m].at[gi, rows(s, F, F)], w_send.at[m, d], w_recv.at[m, s], {"fs": d}
        )

    def spread(block, s, up, down, act_on, own=False):
        src, place, ssem, rsem, after = block
        at = place(s)

        def hop(way, dev):
            act_on(rdma(src if own else at, at, ssem.at[s, way], rsem.at[s], {"fs": dev}))

        if up:
            pl.when(zi < Z - 1)(lambda: hop(0, si + Y))
        if down:
            pl.when(zi > 0)(lambda: hop(1, si - Y))

        def across(k):
            y = lax.rem(yi + k, Y)
            hop(2 + y, zi * Y + y)

        each(1, Y, across)

    def shx_copy(m, s, g, dev):
        at = sh_place(m, s, g)
        return rdma(at, at, shx_send.at[m, s, dev], shx_recv.at[m, s, g], {"gr": dev})

    def arrive(block, s):
        src, place, ssem, rsem, after = block
        rdma(place(s), place(s), ssem.at[s, 0], rsem.at[s], {"fs": fs_peer(1)}).wait_recv()
        if after is not None:
            after(s)

    def start(c):
        c.start()

    def sent(c):
        c.wait_send()

    def relay(block, step, act_on=start):
        def from_below():
            s = si - step * Y
            if act_on is start:
                arrive(block, s)
            spread(block, s, True, False, act_on)

        def from_above():
            s = si + step * Y
            if act_on is start:
                arrive(block, s)
            spread(block, s, False, True, act_on)

        pl.when(zi >= step)(from_below)
        pl.when(zi + step < Z)(from_above)

    def others_arrive(block, step):
        def at(z):
            each(1, Y, lambda k: arrive(block, z * Y + lax.rem(yi + k, Y)))

        if step == 0:
            at(zi)
        else:
            pl.when(zi >= step)(lambda: at(zi - step))
            pl.when(zi + step < Z)(lambda: at(zi + step))

    def block_sent(block):
        spread(block, si, True, True, sent, own=True)
        for step in range(1, Z):
            relay(block, step, sent)

    def sh_place(m, s, g):
        return shn[m].at[rows(s, SF, SF), rows(g, C // G, C // G)]

    def sh_block(m):
        return (
            sh[m].at[:, rows(gi, C // G, C // G)],
            lambda s: sh_place(m, s, gi),
            sh_send.at[m],
            sh_recv.at[m],
            lambda s: each(1, G, lambda j: shx_copy(m, s, gi, gr_peer(j)).start()),
        )

    tok_block = (tok, lambda s: xs.at[rows(s, T, T)], tok_send, tok_recv, None)
    sh_blocks = [sh_block(m) for m in range(3)]

    def shared_step(step):
        for block in sh_blocks:
            if step < Z:
                relay(block, step)
            others_arrive(block, step - 1)

    def x_copy(m, s, g, dev, own=False):
        place = new[m].at[g, rows(s, F, F)]
        src = w[m].at[s] if own else place
        return rdma(src, place, x_send.at[m, s, dev], x_recv.at[m, s, g], {"gr": dev})

    def local_copies():
        return (
            [pltpu.make_async_copy(w[m].at[si], new[m].at[gi, rows(si, F, F)], local_sem.at[m]) for m in range(3)]
            + [pltpu.make_async_copy(sh[m], shn[m].at[rows(si, SF, SF)], local_sem.at[3 + m]) for m in range(3)]
            + [pltpu.make_async_copy(tok, xs.at[rows(si, T, T)], local_sem.at[6])]
        )

    def send_weight(m):
        each(1, S, lambda k: w_copy(m, fs_peer(k), si).start())

    for m in range(3):
        each(1, G, lambda j, m=m: x_copy(m, si, gi, gr_peer(j), own=True).start())
    spread(tok_block, si, True, True, start, own=True)
    send_weight(0)
    for copy in local_copies():
        copy.start()

    def forward(m, lo=1, hi=S):
        def one(k):
            s = fs_from(k)
            w_copy(m, s, s).wait_recv()
            each(1, G, lambda j: x_copy(m, s, gi, gr_peer(j)).start())

        each(lo, hi, one)

    def x_arrive(m, g):
        each(0, S, lambda s: x_copy(m, s, g, g).wait_recv())

    def p_copy(j, t, s):
        return rdma(
            pout.at[j if slots > 1 else 0, t], pin.at[j, s], p_send.at[j, t], p_recv.at[j, s], {"tp": t}
        )

    def a_copy(j, t, s):
        place = act.at[j, rows(s, NH, NH)]
        return rdma(place, place, a_send.at[j, t], a_recv.at[j, s], {"tp": t})

    def first_matmuls(j):
        g = gr_peer(j)
        slot = j if slots > 1 else 0
        for q in range(TP):
            t = tp_peer(1 + q)

            def block(b, t=t):
                x = xs[rows(t * NB + b, T, T), 0:C]
                for m in range(2):
                    part = lax.dot_general(
                        x, new[m][g], (((1,), (1,)), ((), ())), preferred_element_type=jnp.float32
                    )
                    pout[slot, t, rows(b, T, T), m * H : (m + 1) * H] = part.astype(jnp.bfloat16)

            each(0, NB, block)
            if q < TP - 1:
                p_copy(j, t, ti).start()

    def activations(j):
        g = gr_peer(j)
        slot = j if slots > 1 else 0
        expert = g * S + si
        for q in range(1, TP):
            t = tp_peer(q)
            p_copy(j, t, t).wait_recv()

        def block(b):
            r = rows(b, T, T)
            pre = pout[slot, ti, r, :].astype(jnp.float32)
            for q in range(1, TP):
                pre = pre + pin[j, tp_peer(q), r, :].astype(jnp.float32)
            at = rows(ti * NB + b, T, T)
            coded = xs[at, C:].astype(jnp.float32)
            lane = lax.broadcasted_iota(jnp.int32, coded.shape, 1)
            share = jnp.sum(
                jnp.where((lane == expert) | (lane == expert + E), coded, 0.0), axis=1, keepdims=True
            )
            value = silu(pre[:, :H]) * pre[:, H:] * share
            act[j, at, :] = value.astype(jnp.bfloat16)

        each(0, NB, block)
        for q in range(1, TP):
            a_copy(j, tp_peer(q), ti).start()

    if Z > 1:
        relay(tok_block, 1)
    send_weight(1)
    forward(0)
    for step in range(2, Z):
        relay(tok_block, step)
    send_weight(2)
    for block in sh_blocks:
        spread(block, si, True, True, start, own=True)
    forward(1)
    for copy in local_copies():
        copy.wait()
    for step in range(Z):
        others_arrive(tok_block, step)
    for j in range(G):
        if j > 0:
            for m in range(2):
                x_arrive(m, gr_peer(j))
            if slots == 1:
                for q in range(1, TP):
                    p_copy(j - 1, tp_peer(q), ti).wait_send()
        first_matmuls(j)
        if j == 1:
            forward(2, S // 2, S)
        activations(j)
        if j == 0:
            forward(2, 1, S // 2 if G > 1 else S)
    shared_step(1)

    for m in range(2):
        pltpu.make_async_copy(new[m], outs[m], out_sem.at[m]).start()
    for j in range(1, G):
        x_arrive(2, gr_peer(j))
    pltpu.make_async_copy(new[2], outs[2], out_sem.at[2]).start()

    def ry_copy(z, y, src):
        return rdma(
            oz.at[rows(z * Y + y, T, T)],
            rety.at[z, src],
            ry_send.at[z, y],
            ry_recv.at[z, src],
            {"fs": zi * Y + y},
        )

    def r_copy(z, up, dist):
        slot = Z if dist == 1 and not up else z
        return rdma(
            oz.at[rows(z * Y + yi, T, T)],
            ret.at[slot],
            r_send.at[z],
            r_recv.at[slot],
            {"fs": si + Y if up else si - Y},
        )

    def far_first(fn):
        for dist in range(Z - 1, -1, -1):
            pl.when(zi + dist < Z)(functools.partial(fn, zi + dist, True, dist))
            if dist:
                pl.when(zi >= dist)(functools.partial(fn, zi - dist, False, dist))

    for q in range(1, TP):
        for j in range(G):
            a_copy(j, tp_peer(q), tp_peer(q)).wait_recv()

    def down_block(z, up, dist):
        def column(k):
            y = lax.rem(yi + k, Y)
            at = rows(z * Y + y, T, T)
            total = jnp.zeros((T, C), jnp.float32)
            for j in range(G):
                total = total + jnp.dot(
                    act[j, at, :], new[2][gr_peer(j)], preferred_element_type=jnp.float32
                )
            oz[at, :] = total.astype(jnp.bfloat16)
            pl.when(y != yi)(lambda: ry_copy(z, y, yi).start())

        each(1, Y + 1, column)

    far_first(down_block)
    if Z > 1:
        shared_step(2)

    def add_far(z, slot):
        at = rows(z * Y + yi, T, T)
        rdma(
            ret.at[slot], ret.at[slot], r_send.at[z], r_recv.at[slot], {"fs": fs_peer(1)}
        ).wait_recv()
        total = oz[at, :].astype(jnp.float32) + ret[slot].astype(jnp.float32)
        oz[at, :] = total.astype(jnp.bfloat16)

    def column_sum(z, up, dist):
        at = rows(z * Y + yi, T, T)
        total = oz[at, :].astype(jnp.float32)
        for k in range(1, Y):
            y = lax.rem(yi + k, Y)
            ry_copy(z, y, y).wait_recv()
            total = total + rety[z, y].astype(jnp.float32)
        oz[at, :] = total.astype(jnp.bfloat16)
        if dist == 0 or up:
            pl.when(zi > 0)(lambda: add_far(z, z))
        if dist == 0:
            pl.when(zi < Z - 1)(lambda: add_far(z, Z))
        elif not up:
            pl.when(zi < Z - 1)(lambda: add_far(z, z))
        if dist:
            r_copy(z, up, dist).start()

    far_first(column_sum)
    for step in range(3, Z + 1):
        shared_step(step)

    def shared_arrive(m):
        each(
            1,
            S,
            lambda k: each(
                1, G, lambda j: shx_copy(m, fs_from(k), gr_peer(j), gr_peer(j)).wait_recv()
            ),
        )

    def ps_copy(t, s):
        return rdma(psh, pshin.at[s], ps_send.at[t], ps_recv.at[s], {"tp": t})

    for m in range(2):
        shared_arrive(m)
        part = lax.dot_general(
            xs[rows(si, T, T), 0:C],
            shn[m][...],
            (((1,), (1,)), ((), ())),
            preferred_element_type=jnp.float32,
        )
        psh[:, m * SH : (m + 1) * SH] = part.astype(jnp.bfloat16)
        pltpu.make_async_copy(shn[m], shouts[m], out_sem.at[3 + m]).start()
    for q in range(1, TP):
        ps_copy(tp_peer(q), ti).start()
    shared_arrive(2)
    pltpu.make_async_copy(shn[2], shouts[2], out_sem.at[5]).start()
    pre = psh[...].astype(jnp.float32)
    for q in range(1, TP):
        t = tp_peer(q)
        ps_copy(t, t).wait_recv()
        pre = pre + pshin[t].astype(jnp.float32)
    shared_act = (silu(pre[:, :SH]) * pre[:, SH:]).astype(jnp.bfloat16)
    total = jnp.dot(shared_act, shn[2][...], preferred_element_type=jnp.float32)
    total = total + oz[rows(si, T, T), :].astype(jnp.float32)
    mixed[...] = total.astype(jnp.bfloat16)

    for m in range(3):
        pltpu.make_async_copy(new[m], outs[m], out_sem.at[m]).wait()
        pltpu.make_async_copy(shn[m], shouts[m], out_sem.at[3 + m]).wait()
        each(1, S, lambda k, m=m: w_copy(m, fs_peer(k), si).wait_send())
        block_sent(sh_blocks[m])
        each(
            1,
            S,
            lambda k, m=m: each(
                1, G, lambda j: shx_copy(m, fs_from(k), gi, gr_peer(j)).wait_send()
            ),
        )
        each(0, S, lambda s, m=m: each(1, G, lambda j: x_copy(m, s, gi, gr_peer(j)).wait_send()))
    block_sent(tok_block)
    each(0, Z, lambda z: each(1, Y, lambda k: ry_copy(z, lax.rem(yi + k, Y), yi).wait_send()))

    def r_sent(z, up, dist):
        if dist:
            r_copy(z, up, dist).wait_send()

    far_first(r_sent)
    for q in range(1, TP):
        t = tp_peer(q)
        ps_copy(t, ti).wait_send()
        for j in range(G):
            if slots > 1 or j == G - 1:
                p_copy(j, t, ti).wait_send()
            a_copy(j, t, ti).wait_send()


def body(
    Y,
    tokens,
    expert_ids,
    route_weight,
    norm_gain,
    expert_gate,
    expert_up,
    expert_down,
    shared_gate,
    shared_up,
    shared_down,
):
    G, S, TP = lax.axis_size("gr"), lax.axis_size("fs"), lax.axis_size("tp")
    T, C = tokens.shape[0], expert_gate.shape[2]
    F, SF = expert_gate.shape[1], shared_gate.shape[0]
    H, SH = F * S, SF * S
    E, N = G * S, S * T
    NH = N // TP
    lanes = -(-2 * E // 128) * 128
    bf16 = jnp.bfloat16

    tok_float = tokens.astype(jnp.float32)
    normed = (
        tok_float * lax.rsqrt(jnp.mean(tok_float * tok_float, axis=1, keepdims=True) + norm_eps)
    ).astype(bf16)
    normed_cols = lax.dynamic_slice_in_dim(normed, lax.axis_index("tp") * C, C, 1)
    share = route_weight / jnp.sum(route_weight, axis=1, keepdims=True) * route_scale
    lane = jnp.arange(lanes, dtype=jnp.int32)[None, None, :]
    dense = jnp.sum(
        jnp.where(expert_ids[:, :, None] == lane % E, share[:, :, None], 0.0), axis=1
    )
    high = dense.astype(bf16)
    low = (dense - lax.reduce_precision(dense, 8, 7)).astype(bf16)
    place = lane[0]
    coded = jnp.where(place < E, high, jnp.where(place < 2 * E, low, 0))
    payload = jnp.concatenate([normed_cols, coded.astype(bf16)], axis=1)

    weights = (
        fold_gain(expert_gate, norm_gain),
        fold_gain(expert_up, norm_gain),
        expert_down.astype(bf16),
    )
    shared = (
        fold_gain(shared_gate, norm_gain),
        fold_gain(shared_up, norm_gain),
        shared_down.astype(bf16),
    )
    row_bytes = 2 * (2 * G * 2 * H + G * H + 3 * C + lanes)
    slots = G if N * row_bytes < vmem_bytes * 3 // 5 else 1
    dims = (G, S, TP, T, C, H, F, SF, slots, Y)
    vmem, hbm = pl.BlockSpec(memory_space=pltpu.VMEM), pl.BlockSpec(memory_space=pl.ANY)
    dma = pltpu.SemaphoreType.DMA
    results = pl.pallas_call(
        functools.partial(handover, dims),
        out_shape=[jax.ShapeDtypeStruct((T, C), bf16)]
        + [jax.ShapeDtypeStruct((G, H, C), bf16)] * 3
        + [jax.ShapeDtypeStruct((SH, C), bf16)] * 3,
        in_specs=[vmem] * 7,
        out_specs=[vmem] + [hbm] * 6,
        scratch_shapes=[pltpu.VMEM((G, H, C), bf16)] * 3
        + [pltpu.VMEM((SH, C), bf16)] * 3
        + [
            pltpu.VMEM((N, C + lanes), bf16),
            pltpu.VMEM((slots, TP, NH, 2 * H), bf16),
            pltpu.VMEM((G, TP, NH, 2 * H), bf16),
            pltpu.VMEM((G, N, H), bf16),
            pltpu.VMEM((N, C), bf16),
            pltpu.VMEM((S // Y, Y, T, C), bf16),
            pltpu.VMEM((S // Y + 1, T, C), bf16),
            pltpu.VMEM((T, 2 * SH), bf16),
            pltpu.VMEM((TP, T, 2 * SH), bf16),
            dma((7,)),
            dma((6,)),
            dma((S, 2 + Y)),
            dma((S,)),
            dma((3, S)),
            dma((3, S)),
            dma((3, S, G)),
            dma((3, S, G)),
            dma((3, S, 2 + Y)),
            dma((3, S)),
            dma((3, S, G)),
            dma((3, S, G)),
            dma((G, TP)),
            dma((G, TP)),
            dma((G, TP)),
            dma((G, TP)),
            dma((S // Y, Y)),
            dma((S // Y, Y)),
            dma((S // Y,)),
            dma((S // Y + 1,)),
            dma((TP,)),
            dma((TP,)),
        ],
        compiler_params=pltpu.CompilerParams(
            collective_id=0, has_side_effects=True, vmem_limit_bytes=vmem_bytes
        ),
        name="handover",
    )(payload, *weights, *shared)
    mixed = results[0]
    whole = [r.reshape(G, 1, H, C) for r in results[1:4]]
    return (mixed, *whole, *results[4:])


def line_length(mesh):
    places = [d.coords for d in mesh.devices[0, :, 0]]
    axis = [i for i in range(3) if places[0][i] != places[1][i]][0]
    count = 0
    for place in places:
        if any(place[i] != places[0][i] for i in range(3) if i != axis):
            break
        count += 1
    return count if len(places) % count == 0 else len(places)


def solution(mesh):
    placed = (
        P(("gr", "fs"), None),
        P(("gr", "fs"), None),
        P(("gr", "fs"), None),
        P("tp"),
        P("gr", "fs", "tp"),
        P("gr", "fs", "tp"),
        P("gr", "fs", "tp"),
        P("fs", "tp"),
        P("fs", "tp"),
        P("fs", "tp"),
    )
    return jax.shard_map(
        functools.partial(body, line_length(mesh)),
        mesh=mesh,
        in_specs=placed,
        out_specs=(
            P(("gr", "fs"), "tp"),
            P(None, "fs", None, "tp"),
            P(None, "fs", None, "tp"),
            P(None, "fs", None, "tp"),
            P(None, "tp"),
            P(None, "tp"),
            P(None, "tp"),
        ),
        check_vma=False,
    )
```

time: 506 us -> 207 us (0.41); the launches traced: 498 us -> 205 us
  waiting for transfers between devices: 279 us -> 0 us
  Pallas kernels: 0 us -> 179 us
  local copies, waits for them, and re-layouts: 108 us -> 14.6 us
  blocking collectives: 33 us -> 0 us
  starting transfers between devices: 24 us -> 0 us
  matrix products: 17.4 us -> 0 us
  between operations: 14.6 us -> 0.74 us
  other arithmetic: 22.9 us -> 11 us
    all_gather x7 -> x0, waiting for transfers between devices: 243 us -> none  [the longest x1 75.8 us: body(): lax.all_gather(fold_gain(shared_up, norm_gain), 'fs', axis=0, tiled=True)]
    pallas_call x0 -> x1, Pallas kernels: none -> 179 us  [body(): pl.pallas_call(functools.partial(handover, dims), out_shape=[jax.ShapeDty...]
    reshape x9 -> x0, local copies, waits for them, and re-layouts: 38.9 us -> none  [the longest x2 12.3 us: body(): padded[slot_token].reshape(group_count, shard_count, capacity, col_width)]
    all_to_all x1 -> x0, blocking collectives: 31 us -> none  [body(): lax.all_to_all(down_round, 'fs', split_axis=0, concat_axis=1, tiled=True)]
    all_to_all x4 -> x0, waiting for transfers between devices: 23.9 us -> none  [the longest x1 23.9 us: body(): lax.all_to_all(up_round, 'fs', split_axis=0, concat_axis=1, tiled=True)]
    all_to_all x4 -> x0, starting transfers between devices: 23 us -> none  [the longest x1 7.44 us: body(): lax.all_to_all(up_round, 'fs', split_axis=0, concat_axis=1, tiled=True)]
    dot_general x4 -> x0, matrix products: 17.4 us -> none  [the longest x1 8.98 us: body(): jnp.einsum('ihd,ird->hir', rows_weight, slot_rows, preferred_element_type...]
    gather x2 -> x0, local copies, waits for them, and re-layouts: 16.3 us -> none  [the longest x1 9.72 us: body(): result_rows[dest].reshape(tok_rows, top_count, col_width)]
  transfers between devices with their start and end apart: 13 -> 0, of which waited for: 9 -> 0; matrix products, arithmetic and copies ran while one was open for 19% -> 0% of each run, Pallas kernels for 0% -> 0%
where the time goes in v1:
time: 207 us; the launch traced here: 205 us
  Pallas kernels  179 us (86%)
  local copies, waits for them, and re-layouts  14.6 us (7%)
  other arithmetic  11 us (5%)
    pallas_call x1, Pallas kernels, body(): pl.pallas_call(functools.partial(handover, dims), out_shape=[jax.ShapeDty...  179 us
    unnamed x28, local copies, waits for them, and re-layouts  14.5 us

profile of v1, /device:TPU:0, one launch (start us, length us, event | category | flops | bytes accessed | tf_op | source)
XLA Modules:
  0.0 205.2 jit_solution(10394341972154389177)
XLA Ops:
  0.6 0.0 copy-start.1
  0.7 1.5 multiply_reduce_fusion
  2.1 0.7 reduce_sum.28
  2.9 0.7 divide_multiply_fusion
  3.6 0.1 copy.23
  3.7 0.8 copy.22
  4.5 0.4 select_reduce_fusion
  5.0 0.0 copy-start
  5.0 1.7 convert_element_type.41.s2
  6.7 1.8 multiply_convert_fusion.2
  8.5 0.0 copy-done.1
  8.5 0.0 copy-start.5
  8.5 1.1 convert_element_type.38.w2
  9.6 0.0 copy-done
  9.6 0.0 copy-start.4
  9.6 0.0 copy-start.9
  9.6 0.1 convert_element_type.32
  9.8 0.1 fusion
  9.9 0.8 pad_maximum_fusion.tok
  10.7 0.0 copy-done.5
  10.7 0.8 copy-done.4
  11.5 0.0 copy-done.9
  11.5 1.9 multiply_convert_fusion
  13.5 178.9 %handover.1 = (bf16[176,1024]{1,0:T(8,128)(2,1)}, bf16[2,512,1024]{2,1,0:T(8,128)(2,1)}, bf16[2,512,1024]{2,1,0:T(8,128)(2,1)}, bf16[2,512,1024]{2,1,0:T(8,128)(...) custom-call(bf16[176,1152]{1,0:T(8,128)(2,1)} %pad_maximum_fusion.tok, ...), custom_call_target="tpu_custom_call" | custom-call | tf_op jit(solution)/shard_map/handover/pallas_call | solution.py:546
  192.3 1.7 copy.34
  194.1 0.0 copy-start.3
  194.1 3.2 %copy.35 = bf16[2,1,512,1024]{3,2,1,0:T(8,128)(2,1)} copy(bf16[2,1,512,1024]{3,2,1,0:T(8,128)(2,1)} %bitcast.11) | data formatting | bytes 4194304
  197.3 0.0 copy-done.3
  197.3 0.0 copy-start.2
  197.3 1.3 copy.36
  198.6 1.0 copy-done.2
  199.7 0.0 copy-start.8
  199.7 1.3 copy.37
  201.0 0.6 copy-done.8
  201.6 0.0 copy-start.7
  201.6 0.0 copy-start.6
  201.6 1.0 copy.38
  202.6 0.6 copy-done.7
  203.2 1.0 copy.39
  204.2 0.0 copy-done.6
  204.2 1.0 copy.40
  (4 shorter events, 0.0 us)
Async XLA Ops:
  0.6 7.9 %copy-start.1 = (f32[8,64,1024]{2,1,0:T(8,128)S(1)}, f32[8,64,1024]{2,1,0:T(8,128)}, u32[]{:S(2)}) copy-start(f32[8,64,1024]{2,1,0:T(8,128)} %param.16) | copy-start | bytes 6291460
  5.0 4.6 %copy-start = (bf16[176,2048]{1,0:T(8,128)(2,1)S(1)}, bf16[176,2048]{1,0:T(8,128)(2,1)}, u32[]{:S(2)}) copy-start(bf16[176,2048]{1,0:T(8,128)(2,1)} %param.10) | copy-start | bytes 2162692
  8.5 2.2 %copy-start.5 = (f32[8,64,1024]{2,1,0:T(8,128)S(1)}, f32[8,64,1024]{2,1,0:T(8,128)}, u32[]{:S(2)}) copy-start(f32[8,64,1024]{2,1,0:T(8,128)} %param.14) | copy-start | bytes 6291460
  9.6 1.9 copy-start.4
  9.6 1.9 copy-start.9
  194.1 3.2 %copy-start.3 = (bf16[2,512,1024]{2,1,0:T(8,128)(2,1)S(1)}, bf16[2,512,1024]{2,1,0:T(8,128)(2,1)}, u32[]{:S(2)}) copy-start(bf16[2,512,1024]{2,1,0:T(8,128)(2,1)} %get-tuple-element.16) | copy-start | bytes 6291460
  197.3 2.3 %copy-start.2 = (bf16[2,512,1024]{2,1,0:T(8,128)(2,1)S(1)}, bf16[2,512,1024]{2,1,0:T(8,128)(2,1)}, u32[]{:S(2)}) copy-start(bf16[2,512,1024]{2,1,0:T(8,128)(2,1)} %get-tuple-element.17) | copy-start | bytes 6291460
  199.7 2.0 copy-start.8
  201.6 1.6 copy-start.7
  201.6 2.6 %copy-start.6 = (bf16[512,1024]{1,0:T(8,128)(2,1)S(1)}, bf16[512,1024]{1,0:T(8,128)(2,1)}, u32[]{:S(2)}) copy-start(bf16[512,1024]{1,0:T(8,128)(2,1)} %get-tuple-element.54) | copy-start | bytes 3145732
